TPU v7x, 128 devices: a whole 4x4x4 slice. The times are simulated.
128 devices in a mesh: sp: 16 (over z, y), tp: 8 (over x, core).
Axes of the slice: x: 4, y: 4, z: 4, core: 2. Of those that a mesh axis runs over, the one named last changes fastest.
Arguments:
- tokens: bfloat16 [6144, 4096], P(('sp', 'tp')), may hold values from -6 to 6
- norm_gain: bfloat16 [4096], replicated, may hold values from 0.099609375 to 1.8984375
- w_pool_in: bfloat16 [4096, 4096], P('sp', 'tp'), may hold values from -0.09375 to 0.09375
- w_mem_in: bfloat16 [4096, 4096], P('sp', 'tp'), may hold values from -0.09375 to 0.09375
- w_input_gate: bfloat16 [4096, 16], replicated, may hold values from -104 to 104
- w_forget_gate: bfloat16 [4096, 16], replicated, may hold values from -0.09375 to 0.09375
- forget_bias: float32 [16], replicated, may hold values from 3 to 13
- forget_extra: float32 [6144, 16], P('sp', 'tp'), may hold values from 0 to 1.5
- conv_weight: bfloat16 [4, 4096], replicated, may hold values from -3 to 3
- query_map: bfloat16 [1024, 4, 4], replicated, may hold values from -3 to 3
- key_map: bfloat16 [1024, 4, 4], replicated, may hold values from -3 to 3
- pool_map: bfloat16 [16, 256, 256], P('tp'), may hold values from -0.375 to 0.375
- pool_gain: bfloat16 [4096], replicated, may hold values from 0.099609375 to 1.8984375
- mem_gain: bfloat16 [4096], replicated, may hold values from 0.099609375 to 1.8984375
- w_out_pool: bfloat16 [4096, 4096], P('tp', 'sp'), may hold values from -0.0625 to 0.0625
- w_out_mem: bfloat16 [4096, 4096], P('tp', 'sp'), may hold values from -0.0625 to 0.0625
Outputs:
- layer_out: bfloat16 [6144, 4096], P(('sp', 'tp'))
All inputs are finite; a program needn't handle non-finite values.
Results may differ from a plain program's by a relative error of at most 0.019.
The roundings to bfloat16 on the way count: a program that leaves them out, or rounds other values in their place, can miss the bound.
Values may be sent and summed in bfloat16 or wider, within the bound.
No kernel may reach another device: no remote copies, remote signals or barrier semaphores. Data moves between devices by JAX's collectives and lax.ppermute only.
A program may use at most 128 MiB of HBM per device.

v0:
```python
import jax
import jax.numpy as jnp
from jax import lax
from jax.sharding import Mesh
from jax.sharding import PartitionSpec as P

D = 4096
HEAD = 256
CONV = 4
BLOCK = 128
MEMORY_HEADS = 16
SP = ("sp_0", "sp_1")
SP_TP = ("sp_0", "sp_1", "tp")
epsilon = 1e-06
windows_all = (2, 4, 8, 16)
highest = lax.Precision.HIGHEST
lowest = -1e30


def rows_first(arrays, axis, dims):
    turned = [jnp.moveaxis(a, dim, 0) for a, dim in zip(arrays, dims)]
    both = jnp.concatenate([t.reshape(len(t), -1) for t in turned], axis=1)
    filled, at, gathered = (lax.all_gather(both, axis, axis=0, tiled=True), 0, [])
    for t, dim in zip(turned, dims):
        piece = filled[:, at : at + t[0].size].reshape(-1, *t.shape[1:])
        gathered.append(jnp.moveaxis(piece, 0, dim))
        at += t[0].size
    return tuple(gathered)


def in_one_piece(arrays, axis, dim, along):
    ends, at = ([], 0)
    for a in arrays[:-1]:
        at += a.shape[along]
        ends.append(at)
    both = jnp.concatenate(arrays, axis=along)
    return tuple(jnp.split(lax.all_gather(both, axis, axis=dim, tiled=True), ends, axis=along))


def passed_along(shard, axis, by):
    devices = lax.axis_size(axis)
    pairs = [(i, i + by) for i in range(devices) if 0 <= i + by < devices]
    return lax.ppermute(shard, axis, pairs)


def neutral_like(shard, identity):
    return jax.tree.map(
        lambda a, e: jnp.broadcast_to(jnp.asarray(e, a.dtype), a.shape), shard, identity
    )


def entering(shard, axes, combine, identity):
    before = start = neutral_like(shard, identity)
    subtotal = shard
    for axis in reversed(axes):
        devices, position = (lax.axis_size(axis), lax.axis_index(axis))
        pieces = jax.tree.map(lambda part: lax.all_gather(part, axis), subtotal)
        inside, subtotal = (start, start)
        for k in range(devices):
            passed = k < position
            subtotal = combine(subtotal, jax.tree.map(lambda part: part[k], pieces))
            inside = jax.tree.map(lambda new, old: jnp.where(passed, new, old), subtotal, inside)
        before = combine(inside, before)
    return before


def cut_along(shard, dim, devices):
    dims = shard.shape
    pieces = shard.reshape(*dims[:dim], devices, dims[dim] // devices, *dims[dim + 1 :])
    return jnp.moveaxis(pieces, dim, 0)


def summed_on_arrival(shard, axis, dim):
    pieces = cut_along(shard, dim, lax.axis_size(axis))
    arrived = lax.all_to_all(pieces, axis, split_axis=0, concat_axis=0, tiled=True)
    return arrived.astype(jnp.float32).sum(axis=0)


def rms_rows(rows, gain):
    values = rows.astype(jnp.float32)
    factor = lax.rsqrt(jnp.mean(values * values, axis=-1, keepdims=True) + epsilon)
    return (values * factor * gain.astype(jnp.float32)).astype(jnp.bfloat16)


def summary_join(earlier, latter):
    decay_first, peak_first, memory_first = earlier
    decay_second, peak_second, memory_second = latter
    peak_joined = jnp.maximum(decay_second + peak_first, peak_second)
    weight_first = jnp.exp(decay_second + peak_first - peak_joined)[..., None, None]
    weight_second = jnp.exp(peak_second - peak_joined)[..., None, None]
    return (
        decay_first + decay_second,
        peak_joined,
        weight_first * memory_first + weight_second * memory_second,
    )


def on_device(
    tokens,
    norm_gain,
    w_pool_in,
    w_mem_in,
    w_input_gate,
    w_forget_gate,
    forget_bias,
    forget_extra,
    conv_weight,
    query_map,
    key_map,
    pool_map,
    pool_gain,
    mem_gain,
    w_out_pool,
    w_out_mem,
):
    tp_index = lax.axis_index("tp")
    sp_index = lax.axis_index(SP)
    own_rows = tokens.shape[0]
    seq_rows = own_rows * lax.axis_size("tp")
    group_count = pool_map.shape[0]
    pool_cols = group_count * HEAD
    head_count = forget_extra.shape[1]
    mem_cols = head_count * HEAD
    blocks = seq_rows // BLOCK
    pool_enter, mem_enter, pool_leave, mem_leave = rows_first(
        (w_pool_in, w_mem_in, w_out_pool, w_out_mem), SP, (0, 0, 1, 1)
    )
    normalized = rms_rows(tokens, norm_gain)
    input_part = jnp.dot(normalized, w_input_gate, preferred_element_type=jnp.float32) * D ** (-0.5)
    forget_part = jnp.dot(normalized, w_forget_gate, preferred_element_type=jnp.float32)
    gate_rows = jnp.concatenate([input_part, forget_part], axis=1).astype(jnp.bfloat16)
    rows_all, gates_all = in_one_piece((normalized, gate_rows), "tp", 0, 1)
    pool_in = jnp.dot(rows_all, pool_enter, preferred_element_type=jnp.float32).astype(jnp.bfloat16)
    mem_in = jnp.dot(rows_all, mem_enter, preferred_element_type=jnp.float32).astype(jnp.bfloat16)
    head_start = tp_index * head_count
    input_pre = lax.dynamic_slice_in_dim(gates_all, head_start, head_count, 1).astype(jnp.float32)
    forget_pre = lax.dynamic_slice_in_dim(
        gates_all, MEMORY_HEADS + head_start, head_count, 1
    ).astype(jnp.float32)
    bias_own = lax.dynamic_slice_in_dim(forget_bias, head_start, head_count, 0)
    log_forget = jax.nn.log_sigmoid(forget_pre + bias_own) - forget_extra
    pool_rim, mem_rim = passed_along(
        (pool_in[seq_rows - 16 :], mem_in[seq_rows - (CONV - 1) :]), SP, 1
    )
    running = jnp.concatenate([pool_rim, pool_in], axis=0).astype(jnp.float32)
    stride_now = 1
    window_sums = []
    for window in windows_all:
        running = running[:-stride_now] + running[stride_now:]
        stride_now = window
        window_sums.append(running[17 - window : 17 - window + seq_rows])
    channel_group = tp_index * group_count + jnp.arange(pool_cols) // HEAD
    window_pick = channel_group % 4
    window_total = window_sums[0]
    for window_index in range(1, 4):
        window_total = jnp.where(
            window_pick == window_index, window_sums[window_index], window_total
        )
    window_len = (2 ** (window_pick + 1)).astype(jnp.float32)
    position = (sp_index * seq_rows + jnp.arange(seq_rows) + 1).astype(jnp.float32)
    counts = jnp.minimum(position[:, None], window_len[None, :])
    centred = (window_total / counts - pool_in.astype(jnp.float32)).astype(jnp.bfloat16)
    grouped = jnp.einsum(
        "tgc,gcd->tgd",
        centred.reshape(seq_rows, group_count, HEAD),
        pool_map,
        preferred_element_type=jnp.float32,
    )
    gain_own = lax.dynamic_slice_in_dim(pool_gain, tp_index * pool_cols, pool_cols, 0).astype(
        jnp.float32
    )
    pool_mixed = (grouped.reshape(seq_rows, pool_cols) * gain_own).astype(jnp.bfloat16)
    mem_ext = jnp.concatenate([mem_rim, mem_in], axis=0).astype(jnp.float32)
    conv_own = lax.dynamic_slice_in_dim(conv_weight, tp_index * mem_cols, mem_cols, 1).astype(
        jnp.float32
    )
    conv_sum = mem_ext[0:seq_rows] * conv_own[0]
    for tap_index in range(1, CONV):
        conv_sum = conv_sum + mem_ext[tap_index : tap_index + seq_rows] * conv_own[tap_index]
    conv_in = jax.nn.silu(conv_sum).astype(jnp.bfloat16)

    def dense_map(map_table):
        own_blocks = lax.dynamic_slice_in_dim(
            map_table, tp_index * (mem_cols // 4), mem_cols // 4, 0
        )
        own_blocks = own_blocks.astype(jnp.float32).reshape(head_count, HEAD // 4, 4, 4)
        spread = jnp.einsum("hbcd,be->hbced", own_blocks, jnp.eye(HEAD // 4, dtype=jnp.float32))
        return spread.reshape(head_count, HEAD, HEAD).astype(jnp.bfloat16)

    conv_heads = conv_in.reshape(seq_rows, head_count, HEAD)
    query_rows = jnp.einsum(
        "thc,hcd->thd", conv_heads, dense_map(query_map), preferred_element_type=jnp.float32
    ).astype(jnp.bfloat16)
    key_rows = jnp.einsum(
        "thc,hcd->thd", conv_heads, dense_map(key_map), preferred_element_type=jnp.float32
    ).astype(jnp.bfloat16)
    query_blocks = query_rows.reshape(blocks, BLOCK, head_count, HEAD)
    key_blocks = key_rows.reshape(blocks, BLOCK, head_count, HEAD)
    value_blocks = mem_in.reshape(blocks, BLOCK, head_count, HEAD)
    forget_blocks = jnp.swapaxes(log_forget.reshape(blocks, BLOCK, head_count), 1, 2)
    input_blocks = jnp.swapaxes(input_pre.reshape(blocks, BLOCK, head_count), 1, 2)
    cumulative = jnp.cumsum(forget_blocks, axis=-1)
    block_total = cumulative[..., -1]
    along_log = block_total[..., None] - cumulative + input_blocks
    along_peak = jnp.max(along_log, axis=-1)
    key_weight = jnp.exp(along_log - along_peak[..., None]) * HEAD ** (-0.5)
    scaled_keys = key_blocks.astype(jnp.float32) * jnp.swapaxes(key_weight, 1, 2)[..., None]
    block_memory = jnp.einsum(
        "nlhd,nlhe->nhde", scaled_keys, value_blocks.astype(jnp.float32), precision=highest
    )
    identity = (
        jnp.zeros((head_count,), jnp.float32),
        jnp.full((head_count,), lowest, jnp.float32),
        jnp.zeros((head_count, HEAD, HEAD), jnp.float32),
    )

    def local_step(summary, block_part):
        return (summary_join(summary, block_part), summary)

    device_summary, prefixes = lax.scan(
        local_step, identity, (block_total, along_peak, block_memory)
    )
    device_decay, device_peak, device_memory = device_summary
    incoming = entering((device_decay, device_peak, device_memory), SP, summary_join, identity)
    incoming_decay, incoming_peak, incoming_memory = incoming
    start_peak = jnp.maximum(incoming_decay, incoming_peak)
    start_memory = jnp.exp(incoming_peak - start_peak)[..., None, None] * incoming_memory
    unused_decay, block_peak, block_state = summary_join(
        (jnp.zeros((head_count,), jnp.float32), start_peak, start_memory), prefixes
    )
    causal_mask = jnp.tril(jnp.ones((BLOCK, BLOCK), dtype=jnp.bool_))
    log_diff = jnp.where(
        causal_mask,
        cumulative[..., :, None] - cumulative[..., None, :] + input_blocks[..., None, :],
        -jnp.inf,
    )
    carry_log = cumulative + block_peak[..., None]
    row_peak = jnp.maximum(jnp.max(log_diff, axis=-1), carry_log)
    scores = jnp.einsum(
        "nlhd,nshd->nhls", query_blocks, key_blocks, preferred_element_type=jnp.float32
    ) * HEAD ** (-0.5)
    block_weights = (jnp.exp(log_diff - row_peak[..., None]) * scores).astype(jnp.bfloat16)
    within_block = jnp.einsum(
        "nhls,nshe->nlhe", block_weights, value_blocks, preferred_element_type=jnp.float32
    )
    carried = jnp.einsum(
        "nlhd,nhde->nlhe", query_blocks.astype(jnp.float32), block_state, precision=highest
    )
    carried = carried * jnp.swapaxes(jnp.exp(carry_log - row_peak), 1, 2)[..., None]
    hidden = (within_block + carried).reshape(seq_rows, head_count, HEAD)
    centre = jnp.mean(hidden, axis=-1, keepdims=True)
    spread_sq = jnp.mean(jnp.square(hidden - centre), axis=-1, keepdims=True)
    normed = ((hidden - centre) * lax.rsqrt(spread_sq + epsilon)).reshape(seq_rows, mem_cols)
    mem_gain_own = lax.dynamic_slice_in_dim(mem_gain, tp_index * mem_cols, mem_cols, 0).astype(
        jnp.float32
    )
    mem_mixed = (normed * mem_gain_own).astype(jnp.bfloat16)
    summed = summed_on_arrival(
        (
            jnp.dot(pool_mixed, pool_leave, preferred_element_type=jnp.float32)
            + jnp.dot(mem_mixed, mem_leave, preferred_element_type=jnp.float32)
        ).astype(jnp.bfloat16),
        "tp",
        0,
    )
    return summed.astype(jnp.bfloat16)


def solution(mesh):
    torus = Mesh(mesh.devices.reshape(4, 4, mesh.shape["tp"]), ("sp_0", "sp_1", "tp"))
    in_specs = (
        P(SP_TP, None),
        P(),
        P(SP, "tp"),
        P(SP, "tp"),
        P(),
        P(),
        P(),
        P(SP, "tp"),
        P(),
        P(),
        P(),
        P("tp", None, None),
        P(),
        P(),
        P("tp", SP),
        P("tp", SP),
    )
    out_specs = P(SP_TP, None)
    return jax.shard_map(
        on_device, mesh=torus, in_specs=in_specs, out_specs=out_specs, check_vma=False
    )
```

profile of v0, /device:TPU:1, one launch (start us, length us, event | category | flops | bytes accessed | tf_op | source)
XLA Modules:
  0.0 330.2 jit_solution(7433710073949216774)
XLA Ops:
  6.6 0.8 convert_element_type.112
  7.4 1.2 fusion.47
  8.6 1.2 fusion.49
  9.7 1.1 fusion.46
  11.0 1.1 convolution_convert_fusion.2
  12.2 0.9 concatenate.15
  13.5 1.0 pad_maximum_fusion
  14.7 0.7 dynamic-slice_convert_fusion.1
  15.9 7.8 %fusion.9 = (bf16[2,64,4,64,4]{4,3,2,1,0:T(8,128)(2,1)}, bf16[2,64,4,64,4]{4,3,2,1,0:T(8,128)(2,1)}) fusion(f32[64,2,4,4]{3,2,0,1:T(4,128)S(1)} %copy.147, f32[64,64]{1,0:T(8,128)S(1)} %fusion.104, f32[64,2,4,4]{3,2,0,1:T(4,128)S(1)} %copy.138), kind=kLoop, calls=%fused_computation.19 | loop fusion | flops 524288 | bytes 557056 | tf_op jit(solution)/shard_map/convert_element_type | solution.py:188
  23.7 16.6 %convert_element_type.126 = bf16[2,256,256]{2,1,0:T(8,128)(2,1)S(1)} reshape(bf16[2,64,4,64,4]{4,3,2,1,0:T(8,128)(2,1)} %get-tuple-element.196) | data formatting | bytes 524288 | tf_op jit(solution)/shard_map/convert_element_type | solution.py:188
  40.4 17.2 %convert_element_type.135 = bf16[2,256,256]{2,1,0:T(8,128)(2,1)} reshape(bf16[2,64,4,64,4]{4,3,2,1,0:T(8,128)(2,1)} %get-tuple-element.195) | data formatting | bytes 524288 | tf_op jit(solution)/shard_map/convert_element_type | solution.py:188
  60.7 1.4 dynamic-slice_convert_fusion.4
  62.0 0.7 dynamic-slice_convert_fusion.2
  63.4 0.9 split.9
  64.6 0.9 reduce_window_sum.11
  66.1 99.1 %all-gather.12.cloned.1.call-done = bf16[4096,2048]{0,1:T(8,128)(2,1)} async-done(((bf16[256,2048]{0,1:T(8,128)(2,1)}), bf16[4096,2048]{0,1:T(8,128)(2,1)}) %all-gather.12.cloned.1.call-update) | async-done | bytes 16777232 | tf_op jit(solution)/shard_map/all_gather | solution.py:23
  165.2 5.0 %fusion.37 = bf16[384,512]{1,0:T(8,128)(2,1)S(1)} fusion(bf16[4096,2048]{0,1:T(8,128)(2,1)} %all-gather.12.cloned.1.call-done, bf16[384,4128]{1,0:T(8,128)(2,1)} %all-gather.10.cloned.1.call-done), kind=kOutput, calls=%fused_computation.41 | convolution fusion | flops 1610809344 | bytes 7733248 | tf_op jit(solution)/shard_map/dot_general | solution.py:134
  170.2 2.8 collective-permute-start.1
  175.0 0.9 fusion.58
  176.0 16.5 %while.21 = (s32[]{:T(128)}, f32[2]{0:T(128)}, f32[2]{0:T(128)S(1)}, f32[2,256,256]{2,1,0:T(8,128)S(1)}, f32[3,2]{1,0:T(4,128)}, /*index=5*/f32[3,2]{1,0:T(4,128...) while((s32[]{:T(128)}, f32[2]{0:T(128)}, ...), condition=%wide.region_5.6_spmd.clone, body=%wide.region_4.5_spmd.clone.sunk | while | flops 655377 | bytes 2622245 | solution.py:220
  176.0 1.3 subtract_exponential_fusion.19
  178.0 0.9 bitcast_dynamic-update-slice_fusion.2
  179.0 1.3 dynamic_update_slice.19
  180.2 1.3 dynamic_update_slice.20
  181.5 1.3 subtract_exponential_fusion.19
  183.5 0.8 bitcast_dynamic-update-slice_fusion.2
  184.4 1.3 dynamic_update_slice.19
  185.7 1.3 dynamic_update_slice.20
  187.0 1.3 subtract_exponential_fusion.19
  188.9 0.9 bitcast_dynamic-update-slice_fusion.2
  189.9 1.3 dynamic_update_slice.19
  191.2 1.3 dynamic_update_slice.20
  192.5 0.8 copy-done.1
  193.6 1.1 fusion.91
  194.7 5.0 %fusion.32 = bf16[384,512]{1,0:T(8,128)(2,1)S(1)} fusion(bf16[4096,2048]{0,1:T(8,128)(2,1)} %all-gather.12.cloned.1.call-done, bf16[384,4128]{1,0:T(8,128)(2,1)} %all-gather.10.cloned.1.call-done), kind=kOutput, calls=%fused_computation.40 | convolution fusion | flops 1610809344 | bytes 7733248 | tf_op jit(solution)/shard_map/dot_general | solution.py:133
  200.2 3.4 %collective-permute-start = (bf16[16,512]{1,0:T(8,128)(2,1)S(1)}, bf16[16,512]{1,0:T(8,128)(2,1)S(1)}, u32[]{:S(2)}, u32[]{:S(2)}) collective-permute-start(bf16[16,512]{1,0:T(8,128)(2,1)S(1)} %slice.225), channel_id=1, source_target_pairs={{0,8},{8,16},{16,24},{24,32},{32,40},{40,48},{48,56},{56,64},{64,7... | collective-permute-start | bytes 49160 | tf_op jit(solution)/shard_map/ppermute | solution.py:43
  203.6 11.7 %all-reduce.2 = (f32[8]{0:T(128)S(1)}, f32[8]{0:T(128)S(1)}) all-reduce(f32[8]{0:T(128)S(1)} %dynamic-update-slice.1, f32[8]{0:T(128)S(1)} %dynamic-update-slice), channel_id=3, replica_groups=mesh['sp_0'=4,'sp_1'=4,'tp'=8] {'sp_1'}, use_global_device_ids=true, to_apply=%add.1 | all-reduce | flops 16 | bytes 128
  215.4 6.0 %all-gather.3 = f32[4,1,2]{2,1,0:T(1,128)S(1)} all-gather(f32[1,1,2]{2,1,0:T(1,128)S(1)} %get-tuple-element.225), channel_id=1, replica_groups=mesh['sp_0'=4,'sp_1'=4,'tp'=8] {'sp_0'}, dimensions={0}, use_global_device_ids=true | all-gather | bytes 40 | tf_op jit(solution)/shard_map/all_gather | solution.py:57
  221.4 7.1 %all-gather.4 = f32[4,1,2]{2,1,0:T(1,128)S(1)} all-gather(f32[1,1,2]{2,1,0:T(1,128)S(1)} %get-tuple-element.186), channel_id=1, replica_groups=mesh['sp_0'=4,'sp_1'=4,'tp'=8] {'sp_0'}, dimensions={0}, use_global_device_ids=true | all-gather | bytes 40 | tf_op jit(solution)/shard_map/all_gather | solution.py:57
  230.7 2.6 fusion.74
  233.3 1.4 convolution_bitcast_fusion
  237.5 6.8 %fusion.13 = f32[384,4096]{1,0:T(8,128)} fusion(bf16[384,512]{0,1:T(8,128)(2,1)S(1)} %fusion.57, bf16[4096,2048]{0,1:T(8,128)(2,1)} %all-gather.12.cloned.1.call-done), kind=kOutput, calls=%fused_computation.24 | convolution fusion | flops 1610612736 | bytes 10878976 | tf_op jit(solution)/shard_map/dot_general | solution.py:260
  244.3 23.6 %all-gather.14.cloned.1.call-done = f32[4,2,256,256]{3,2,1,0:T(8,128)} async-done(((f32[1,2,256,256]{3,2,1,0:T(8,128)}), f32[4,2,256,256]{3,2,1,0:T(8,128)}) %all-gather.14.cloned.1.call-update) | async-done | bytes 2097168 | tf_op jit(solution)/shard_map/all_gather | solution.py:57
  267.9 2.4 fusion.69
  270.3 1.6 fusion.141
  274.1 5.9 %add_convert_fusion = bf16[384,4096]{1,0:T(8,128)(2,1)S(1)} fusion(f32[384,4096]{1,0:T(8,128)} %fusion.13, bf16[4096,2048]{0,1:T(8,128)(2,1)} %all-gather.12.cloned.1.call-done, f32[384,512]{1,0:T(8,128)S(1)} %bitcast.394, f32[384,512]{1,0:T(8,128)S(1)} %bitcast.396, f32[384,512]{1,0:T(8,128)S(1)} %bitcast.395, f32[512]{0:T(512)S(1)} %copy-done.15), kind=kOutput, calls=%fused_computation.20 | convolution fusion | flops 1614544896 | bytes 15992832 | tf_op jit(solution)/shard_map/dot_general | solution.py:261
  280.1 42.3 %all_to_all.5 = bf16[8,48,4096]{2,1,0:T(8,128)(2,1)S(1)} all-to-all(bf16[8,48,4096]{2,1,0:T(8,128)(2,1)S(1)} %bitcast.393), channel_id=1, replica_groups=mesh['sp_0'=4,'sp_1'=4,'tp'=8] {'tp'}, dimensions={0} | all-to-all | bytes 6291456 | tf_op jit(solution)/shard_map/all_to_all | solution.py:75
  322.4 1.3 reduce_sum.42
  (168 shorter events, 17.2 us)
Async XLA Ops:
  6.5 230.4 %copy-start = (bf16[2,256,256]{2,1,0:T(8,128)(2,1)S(1)}, bf16[2,256,256]{2,1,0:T(8,128)(2,1)}, u32[]{:S(2)}) copy-start(bf16[2,256,256]{2,1,0:T(8,128)(2,1)} %param.29) | copy-start | bytes 786436
  6.5 6.6 %copy-start.6 = (bf16[256,512]{1,0:T(8,128)(2,1)S(1)}, bf16[256,512]{1,0:T(8,128)(2,1)}, u32[]{:S(2)}) copy-start(bf16[256,512]{1,0:T(8,128)(2,1)} %param.20) | copy-start | bytes 786436
  6.5 6.8 %copy-start.7 = (bf16[256,512]{1,0:T(8,128)(2,1)S(1)}, bf16[256,512]{1,0:T(8,128)(2,1)}, u32[]{:S(2)}) copy-start(bf16[256,512]{1,0:T(8,128)(2,1)} %param.21) | copy-start | bytes 786436
  6.5 6.9 %copy-start.9 = (bf16[512,256]{1,0:T(8,128)(2,1)S(1)}, bf16[512,256]{1,0:T(8,128)(2,1)}, u32[]{:S(2)}) copy-start(bf16[512,256]{1,0:T(8,128)(2,1)} %param.32) | copy-start | bytes 786436
  6.5 6.9 %copy-start.8 = (bf16[512,256]{1,0:T(8,128)(2,1)S(1)}, bf16[512,256]{1,0:T(8,128)(2,1)}, u32[]{:S(2)}) copy-start(bf16[512,256]{1,0:T(8,128)(2,1)} %param.33) | copy-start | bytes 786436
  6.5 56.8 %all-gather.10.cloned.1.call-start = ((), (), s32[]{:S(2)}) async-start(), calls=%async_computation.1 | async-start | bytes 3649536 | tf_op jit(solution)/shard_map/all_gather | solution.py:37
  13.1 152.1 %all-gather.12.cloned.1.call-start = ((), (), s32[]{:S(2)}) async-start(), calls=%async_computation.2 | async-start | bytes 17825792 | tf_op jit(solution)/shard_map/all_gather | solution.py:23
  14.5 216.2 %all-gather.16.cloned.1.call-start = ((), (), s32[]{:S(2)}) async-start(), calls=%async_computation.4 | async-start | bytes 2621440 | tf_op jit(solution)/shard_map/all_gather | solution.py:57
  40.3 17.3 %copy-start.34 = (f32[16]{0:T(128)S(1)}, f32[16]{0:T(128)}, u32[]{:S(2)}) copy-start(f32[16]{0:T(128)} %param.24) | copy-start | bytes 196
  40.4 17.3 %copy-start.35 = (u32[128]{0:T(128)S(1)}, u32[128]{0:T(128)}, u32[]{:S(2)}) copy-start(u32[128]{0:T(128)} %constant.147) | copy-start | bytes 1540
  40.4 24.1 %copy-start.30 = (f32[384,2]{0,1:T(2,128)S(1)}, f32[384,2]{0,1:T(2,128)}, u32[]{:S(2)}) copy-start(f32[384,2]{0,1:T(2,128)} %param.25) | copy-start | bytes 9220
  65.8 107.2 %copy-start.14 = (f32[3,2]{1,0:T(4,128)}, f32[3,2]{1,0:T(4,128)S(1)}, u32[]{:S(2)}) copy-start(f32[3,2]{1,0:T(4,128)S(1)} %copy.146) | copy-start | bytes 76
  65.9 107.1 %copy-start.11 = (f32[384,2]{0,1:T(2,128)}, f32[384,2]{0,1:T(2,128)S(1)}, u32[]{:S(2)}) copy-start(f32[384,2]{0,1:T(2,128)S(1)} %copy.173) | copy-start | bytes 9220
  66.1 106.9 %copy-start.13 = (f32[3,2]{1,0:T(4,128)}, f32[3,2]{1,0:T(4,128)S(1)}, u32[]{:S(2)}) copy-start(f32[3,2]{1,0:T(4,128)S(1)} %add_reduce_fusion) | copy-start | bytes 76
  170.2 3.7 %collective-permute-start.1 = (bf16[3,512]{1,0:T(4,128)(2,1)S(1)}, bf16[3,512]{1,0:T(4,128)(2,1)S(1)}, u32[]{:S(2)}, u32[]{:S(2)}) collective-permute-start(bf16[3,512]{1,0:T(4,128)(2,1)S(1)} %slice.242), channel_id=1, source_target_pairs={{0,8},{8,16},{16,24},{24,32},{32,40},{40,48},{48,56},{56,64},{64,7... | collective-permute-start | bytes 9224 | tf_op jit(solution)/shard_map/ppermute | solution.py:43
  192.5 0.8 copy-start.1
  193.3 74.6 %all-gather.14.cloned.1.call-start = ((), (), s32[]{:S(2)}) async-start(), calls=%async_computation.3 | async-start | bytes 2621440 | tf_op jit(solution)/shard_map/all_gather | solution.py:57
  194.6 5.1 %copy-start.16 = (f32[2]{0:T(128)S(1)}, f32[2]{0:T(128)}, u32[]{:S(2)}) copy-start(f32[2]{0:T(128)} %get-tuple-element.63) | copy-start | bytes 28
  194.6 33.9 %copy-start.4 = (bf16[2,256,256]{2,1,0:T(8,128)(2,1)S(1)}, bf16[2,256,256]{2,1,0:T(8,128)(2,1)}, u32[]{:S(2)}) copy-start(bf16[2,256,256]{2,1,0:T(8,128)(2,1)} %convert_element_type.135) | copy-start | bytes 786436
  194.6 34.5 %copy-start.20 = (f32[3,2]{1,0:T(4,128)S(1)}, f32[3,2]{1,0:T(4,128)}, u32[]{:S(2)}) copy-start(f32[3,2]{1,0:T(4,128)} %get-tuple-element.65) | copy-start | bytes 76
  194.6 34.5 %copy-start.31 = (f32[3,2]{1,0:T(4,128)S(1)}, f32[3,2]{1,0:T(4,128)}, u32[]{:S(2)}) copy-start(f32[3,2]{1,0:T(4,128)} %get-tuple-element.62) | copy-start | bytes 76
  199.7 33.6 %copy-start.10 = (pred[128,128]{1,0:T(8,128)(4,1)S(1)}, pred[128,128]{1,0:T(8,128)(4,1)}, u32[]{:S(2)}) copy-start(pred[128,128]{1,0:T(8,128)(4,1)} %iota_compare_fusion) | copy-start | bytes 49156
  199.7 33.6 %copy-start.12 = (f32[384,2]{0,1:T(2,128)S(1)}, f32[384,2]{0,1:T(2,128)}, u32[]{:S(2)}) copy-start(f32[384,2]{0,1:T(2,128)} %copy-done.11) | copy-start | bytes 9220
  200.2 35.1 %collective-permute-start = (bf16[16,512]{1,0:T(8,128)(2,1)S(1)}, bf16[16,512]{1,0:T(8,128)(2,1)S(1)}, u32[]{:S(2)}, u32[]{:S(2)}) collective-permute-start(bf16[16,512]{1,0:T(8,128)(2,1)S(1)} %slice.225), channel_id=1, source_target_pairs={{0,8},{8,16},{16,24},{24,32},{32,40},{40,48},{48,56},{56,64},{64,7... | collective-permute-start | bytes 49160 | tf_op jit(solution)/shard_map/ppermute | solution.py:43
  230.5 4.9 %copy-start.21 = (f32[2]{0:T(128)}, f32[2]{0:T(128)S(1)}, u32[]{:S(2)}) copy-start(f32[2]{0:T(128)S(1)} %get-tuple-element.215) | copy-start | bytes 28
  230.5 4.9 %copy-start.23 = (f32[2]{0:T(128)}, f32[2]{0:T(128)S(1)}, u32[]{:S(2)}) copy-start(f32[2]{0:T(128)S(1)} %get-tuple-element.216) | copy-start | bytes 28
  230.5 4.9 %copy-start.24 = (f32[2]{0:T(128)}, f32[2]{0:T(128)S(1)}, u32[]{:S(2)}) copy-start(f32[2]{0:T(128)S(1)} %get-tuple-element.217) | copy-start | bytes 28
  230.5 4.9 %copy-start.25 = (f32[2]{0:T(128)}, f32[2]{0:T(128)S(1)}, u32[]{:S(2)}) copy-start(f32[2]{0:T(128)S(1)} %get-tuple-element.218) | copy-start | bytes 28
  230.5 4.9 %copy-start.26 = (f32[2]{0:T(128)}, f32[2]{0:T(128)S(1)}, u32[]{:S(2)}) copy-start(f32[2]{0:T(128)S(1)} %get-tuple-element.219) | copy-start | bytes 28
  230.5 4.9 %copy-start.27 = (f32[2]{0:T(128)}, f32[2]{0:T(128)S(1)}, u32[]{:S(2)}) copy-start(f32[2]{0:T(128)S(1)} %get-tuple-element.220) | copy-start | bytes 28
  230.5 4.9 %copy-start.28 = (f32[2]{0:T(128)}, f32[2]{0:T(128)S(1)}, u32[]{:S(2)}) copy-start(f32[2]{0:T(128)S(1)} %get-tuple-element.221) | copy-start | bytes 28
  230.5 4.9 %copy-start.29 = (f32[2]{0:T(128)}, f32[2]{0:T(128)S(1)}, u32[]{:S(2)}) copy-start(f32[2]{0:T(128)S(1)} %get-tuple-element.222) | copy-start | bytes 28
  235.7 0.7 copy-start.17
  235.7 0.7 copy-start.18
  235.7 0.7 copy-start.32
  235.7 0.7 copy-start.33
  236.1 1.2 copy-start.19
  237.5 30.4 %copy-start.2 = (f32[8,256,256]{2,1,0:T(8,128)S(1)}, f32[8,256,256]{2,1,0:T(8,128)}, u32[]{:S(2)}) copy-start(f32[8,256,256]{2,1,0:T(8,128)} %all-gather.16.cloned.1.call-done) | copy-start | bytes 6291460
  237.5 30.4 %copy-start.22 = (f32[2]{0:T(128)S(1)}, f32[2]{0:T(128)}, u32[]{:S(2)}) copy-start(f32[2]{0:T(128)} %copy-done.21) | copy-start | bytes 28
  244.3 26.0 %copy-start.5 = (f32[3,128,2,256]{1,3,2,0:T(8,128)S(1)}, f32[3,128,2,256]{1,3,2,0:T(8,128)}, u32[]{:S(2)}) copy-start(f32[3,128,2,256]{1,3,2,0:T(8,128)} %convolution_bitcast_fusion) | copy-start | bytes 2359300
  267.9 2.4 copy-start.3
  273.3 0.8 copy-start.15
Sparse Core Ops, SparseCore 0:
  13.2 31.6 all-gather.9
  47.0 118.1 all-gather.11
  193.4 34.3 all-gather.15
  233.4 34.4 all-gather.13
where the time goes:
time: 331 us; the launch traced here: 330 us
  waiting for transfers between devices  123 us (37%)
  blocking collectives  67.1 us (20%)
  local copies, waits for them, and re-layouts  50.4 us (15%)
  other arithmetic  38.8 us (12%)
  matrix products  29.9 us (9%)
  between operations  14.6 us (4%)
  starting transfers between devices  6.58 us (2%)
    all_gather x1, waiting for transfers between devices, rows_first(): lax.all_gather(both, axis, axis=0, tiled=True)  99.1 us
    all_to_all x1, blocking collectives, summed_on_arrival(): lax.all_to_all(pieces, axis, split_axis=0, concat_axis=0, tiled=True)  42.3 us
    convert_element_type x2, local copies, waits for them, and re-layouts, dense_map(): return spread.reshape(head_count, HEAD, HEAD).astype(jnp.bfloat16)  33.8 us
    all_gather x2, waiting for transfers between devices, entering(): pieces = jax.tree.map(lambda part: lax.all_gather(part, axis), subtotal)  23.6 us
    all_gather x2, blocking collectives, entering(): pieces = jax.tree.map(lambda part: lax.all_gather(part, axis), subtotal)  13.1 us
    unnamed x1, blocking collectives  11.7 us
    convert_element_type x1, other arithmetic, dense_map(): return spread.reshape(head_count, HEAD, HEAD).astype(jnp.bfloat16)  7.81 us
    dynamic_update_slice x6, local copies, waits for them, and re-layouts, on_device(): lax.scan(local_step, identity, (block_total, along_peak, block_memory))  7.64 us
  transfers between devices with their start and end apart: 6, of which 2 were waited for; matrix products, arithmetic and copies ran while one was open for 23% of the time, Pallas kernels for 0%

commit v1 on v0

--- a/solution.py
+++ b/solution.py
@@ -20,7 +20,14 @@
 def rows_first(arrays, axis, dims):
     turned = [jnp.moveaxis(a, dim, 0) for a, dim in zip(arrays, dims)]
     both = jnp.concatenate([t.reshape(len(t), -1) for t in turned], axis=1)
-    filled, at, gathered = (lax.all_gather(both, axis, axis=0, tiled=True), 0, [])
+
+    def point_recast(z):
+        taken_in = jnp.stack([z for _ in range(lax.axis_size(axis))])
+        mid_arr = lax.all_to_all(taken_in, axis, 0, 0)
+        opened = jnp.concatenate(mid_arr, axis=0)
+        return opened
+
+    filled, at, gathered = (point_recast(both), 0, [])
     for t, dim in zip(turned, dims):
         piece = filled[:, at : at + t[0].size].reshape(-1, *t.shape[1:])
         gathered.append(jnp.moveaxis(piece, 0, dim))

time: 331 us -> 440 us (1.33)
  waiting for transfers between devices: 123 us -> 220 us
  local copies, waits for them, and re-layouts: 50.4 us -> 59.1 us
  starting transfers between devices: 6.58 us -> 13.8 us
    all_to_all x0 -> x1, waiting for transfers between devices: none -> 196 us  [point_recast(): mid_arr = lax.all_to_all(taken_in, axis, 0, 0)]
    all_gather x1 -> x0, waiting for transfers between devices: 99.1 us -> none  [rows_first(): lax.all_gather(both, axis, axis=0, tiled=True)]
    all_to_all x0 -> x1, starting transfers between devices: none -> 8.78 us  [point_recast(): mid_arr = lax.all_to_all(taken_in, axis, 0, 0)]
    another operation x6 -> x7, local copies, waits for them, and re-layouts: 0.72 us -> 6.74 us  [the longest x1 6.02 us: point_recast(): taken_in = jnp.stack([z for _ in range(lax.axis_size(axis))])]
  transfers between devices with their start and end apart: 6 -> 6, of which waited for: 2 -> 2; matrix products, arithmetic and copies ran while one was open for 23% -> 17% of each run, Pallas kernels for 0% -> 0%
where the time goes in v1:
time: 440 us; the launch traced here: 439 us
  waiting for transfers between devices  220 us (50%)
  blocking collectives  67.2 us (15%)
  local copies, waits for them, and re-layouts  59.1 us (13%)
  other arithmetic  36 us (8%)
  matrix products  28 us (6%)
  between operations  14.6 us (3%)
  starting transfers between devices  13.8 us (3%)
    all_to_all x1, waiting for transfers between devices, point_recast(): mid_arr = lax.all_to_all(taken_in, axis, 0, 0)  196 us
    all_to_all x1, blocking collectives, summed_on_arrival(): lax.all_to_all(pieces, axis, split_axis=0, concat_axis=0, tiled=True)  42.3 us
    convert_element_type x2, local copies, waits for them, and re-layouts, dense_map(): return spread.reshape(head_count, HEAD, HEAD).astype(jnp.bfloat16)  33.8 us
    all_gather x2, waiting for transfers between devices, entering(): pieces = jax.tree.map(lambda part: lax.all_gather(part, axis), subtotal)  24.2 us
    all_gather x2, blocking collectives, entering(): pieces = jax.tree.map(lambda part: lax.all_gather(part, axis), subtotal)  14.3 us
    unnamed x1, blocking collectives  10.5 us
  transfers between devices with their start and end apart: 6, of which 2 were waited for; matrix products, arithmetic and copies ran while one was open for 17% of the time, Pallas kernels for 0%

profile of v1, /device:TPU:1, one launch (start us, length us, event | category | flops | bytes accessed | tf_op | source)
XLA Modules:
  0.0 438.7 jit_solution(4118447603560286749)
XLA Ops:
  6.5 1.1 copy.133
  7.7 1.1 copy.134
  8.8 1.1 pad_maximum_fusion
  10.5 6.0 %stack.2 = bf16[16,256,2048]{2,1,0:T(8,128)(2,1)} broadcast(bf16[256,2048]{1,0:T(8,128)(2,1)S(1)} %copy.135), dimensions={1,2} | broadcast | bytes 17825792 | tf_op jit(solution)/shard_map/stack | solution.py:25
  16.6 8.8 %all-to-all-start = ((bf16[16,256,2048]{2,1,0:T(8,128)(2,1)}), bf16[16,256,2048]{2,1,0:T(8,128)(2,1)}, u32[]{:S(2)}, u32[]{:S(2)}) async-start(bf16[16,256,2048]{2,1,0:T(8,128)(2,1)} %stack.2), calls=%async_computation | async-start | bytes 33554432 | tf_op jit(solution)/shard_map/all_to_all | solution.py:26
  26.4 0.9 concatenate.15
  27.5 0.7 dynamic-slice_convert_fusion.1
  28.7 7.8 %fusion.9 = (bf16[2,64,4,64,4]{4,3,2,1,0:T(8,128)(2,1)}, bf16[2,64,4,64,4]{4,3,2,1,0:T(8,128)(2,1)}) fusion(f32[64,2,4,4]{3,2,0,1:T(4,128)S(1)} %copy.152, f32[64,64]{1,0:T(8,128)S(1)} %fusion.104, f32[64,2,4,4]{3,2,0,1:T(4,128)S(1)} %copy.143), kind=kLoop, calls=%fused_computation.19 | loop fusion | flops 524288 | bytes 557056 | tf_op jit(solution)/shard_map/convert_element_type | solution.py:195
  36.5 16.6 %convert_element_type.126 = bf16[2,256,256]{2,1,0:T(8,128)(2,1)S(1)} reshape(bf16[2,64,4,64,4]{4,3,2,1,0:T(8,128)(2,1)} %get-tuple-element.196) | data formatting | bytes 524288 | tf_op jit(solution)/shard_map/convert_element_type | solution.py:195
  53.2 17.3 %convert_element_type.135 = bf16[2,256,256]{2,1,0:T(8,128)(2,1)} reshape(bf16[2,64,4,64,4]{4,3,2,1,0:T(8,128)(2,1)} %get-tuple-element.195) | data formatting | bytes 524288 | tf_op jit(solution)/shard_map/convert_element_type | solution.py:195
  73.5 1.4 dynamic-slice_convert_fusion.4
  74.8 0.7 dynamic-slice_convert_fusion.2
  76.2 0.9 split.9
  77.4 0.9 reduce_window_sum.11
  78.9 195.6 %all-to-all-done = bf16[16,256,2048]{2,1,0:T(8,128)(2,1)} async-done(((bf16[16,256,2048]{2,1,0:T(8,128)(2,1)}), bf16[16,256,2048]{2,1,0:T(8,128)(2,1)}, u32[]{:S(2)}, u32[]{:S(2)}) %all-to-all-start) | async-done | bytes 16777248 | tf_op jit(solution)/shard_map/all_to_all | solution.py:26
  274.5 4.9 %fusion.37 = bf16[384,512]{1,0:T(8,128)(2,1)S(1)} fusion(bf16[4096,2048]{1,0:T(8,128)(2,1)} %bitcast.2, bf16[384,4128]{1,0:T(8,128)(2,1)} %all-gather.9.cloned.1.call-done), kind=kOutput, calls=%fused_computation.41 | convolution fusion | flops 1610809344 | bytes 7733248 | tf_op jit(solution)/shard_map/dot_general | solution.py:141
  279.4 1.3 collective-permute-start.1
  282.8 0.9 fusion.58
  283.7 16.6 %while.21 = (s32[]{:T(128)}, f32[2]{0:T(128)}, f32[2]{0:T(128)S(1)}, f32[2,256,256]{2,1,0:T(8,128)S(1)}, f32[3,2]{1,0:T(4,128)}, /*index=5*/f32[3,2]{1,0:T(4,128...) while((s32[]{:T(128)}, f32[2]{0:T(128)}, ...), condition=%wide.region_5.6_spmd.clone, body=%wide.region_4.5_spmd.clone.sunk | while | flops 655377 | bytes 2622245 | solution.py:227
  283.7 1.3 subtract_exponential_fusion.19
  285.0 0.7 subtract_exponential_fusion.20
  285.7 0.9 bitcast_dynamic-update-slice_fusion.2
  286.7 1.3 dynamic_update_slice.19
  288.0 1.3 dynamic_update_slice.20
  289.3 1.3 subtract_exponential_fusion.19
  291.2 0.8 bitcast_dynamic-update-slice_fusion.2
  292.2 1.3 dynamic_update_slice.19
  293.5 1.3 dynamic_update_slice.20
  294.8 1.3 subtract_exponential_fusion.19
  296.7 0.9 bitcast_dynamic-update-slice_fusion.2
  297.7 1.3 dynamic_update_slice.19
  299.0 1.3 dynamic_update_slice.20
  300.3 0.8 copy-done.1
  301.4 1.1 fusion.91
  302.5 5.0 %fusion.32 = bf16[384,512]{1,0:T(8,128)(2,1)S(1)} fusion(bf16[4096,2048]{1,0:T(8,128)(2,1)} %bitcast.2, bf16[384,4128]{1,0:T(8,128)(2,1)} %all-gather.9.cloned.1.call-done), kind=kOutput, calls=%fused_computation.40 | convolution fusion | flops 1610809344 | bytes 7733248 | tf_op jit(solution)/shard_map/dot_general | solution.py:140
  307.9 3.4 collective-permute-start
  311.4 10.5 %all-reduce.2 = (f32[8]{0:T(128)S(1)}, f32[8]{0:T(128)S(1)}) all-reduce(f32[8]{0:T(128)S(1)} %dynamic-update-slice.1, f32[8]{0:T(128)S(1)} %dynamic-update-slice), channel_id=3, replica_groups=mesh['sp_0'=4,'sp_1'=4,'tp'=8] {'sp_1'}, use_global_device_ids=true, to_apply=%add.1 | all-reduce | flops 16 | bytes 128
  322.0 8.7 %all-gather.3 = f32[4,1,2]{2,1,0:T(1,128)S(1)} all-gather(f32[1,1,2]{2,1,0:T(1,128)S(1)} %get-tuple-element.225), channel_id=1, replica_groups=mesh['sp_0'=4,'sp_1'=4,'tp'=8] {'sp_0'}, dimensions={0}, use_global_device_ids=true | all-gather | bytes 40 | tf_op jit(solution)/shard_map/all_gather | solution.py:64
  330.7 5.6 %all-gather.4 = f32[4,1,2]{2,1,0:T(1,128)S(1)} all-gather(f32[1,1,2]{2,1,0:T(1,128)S(1)} %get-tuple-element.186), channel_id=1, replica_groups=mesh['sp_0'=4,'sp_1'=4,'tp'=8] {'sp_0'}, dimensions={0}, use_global_device_ids=true | all-gather | bytes 40 | tf_op jit(solution)/shard_map/all_gather | solution.py:64
  338.5 2.6 fusion.74
  341.1 1.4 convolution_bitcast_fusion
  345.3 6.9 %fusion.13 = f32[384,4096]{1,0:T(8,128)} fusion(bf16[384,512]{0,1:T(8,128)(2,1)S(1)} %fusion.57, bf16[4096,2048]{1,0:T(8,128)(2,1)} %bitcast.2), kind=kOutput, calls=%fused_computation.24 | convolution fusion | flops 1610612736 | bytes 10878976 | tf_op jit(solution)/shard_map/dot_general | solution.py:267
  352.1 24.2 %all-gather.11.cloned.1.call-done = f32[4,2,256,256]{3,2,1,0:T(8,128)} async-done(((f32[1,2,256,256]{3,2,1,0:T(8,128)}), f32[4,2,256,256]{3,2,1,0:T(8,128)}) %all-gather.11.cloned.1.call-update) | async-done | bytes 2097168 | tf_op jit(solution)/shard_map/all_gather | solution.py:64
  376.4 2.4 fusion.69
  378.8 1.6 fusion.141
  382.6 5.9 %add_convert_fusion = bf16[384,4096]{1,0:T(8,128)(2,1)S(1)} fusion(f32[384,4096]{1,0:T(8,128)} %fusion.13, bf16[4096,2048]{1,0:T(8,128)(2,1)} %bitcast.2, f32[384,512]{1,0:T(8,128)S(1)} %bitcast.397, f32[384,512]{1,0:T(8,128)S(1)} %bitcast.399, f32[384,512]{1,0:T(8,128)S(1)} %bitcast.398, f32[512]{0:T(512)S(1)} %copy-done.17), kind=kOutput, calls=%fused_computation.20 | convolution fusion | flops 1614544896 | bytes 15992832 | tf_op jit(solution)/shard_map/dot_general | solution.py:268
  388.5 42.3 %all_to_all.10 = bf16[8,48,4096]{2,1,0:T(8,128)(2,1)S(1)} all-to-all(bf16[8,48,4096]{2,1,0:T(8,128)(2,1)S(1)} %bitcast.394), channel_id=1, replica_groups=mesh['sp_0'=4,'sp_1'=4,'tp'=8] {'tp'}, dimensions={0} | all-to-all | bytes 6291456 | tf_op jit(solution)/shard_map/all_to_all | solution.py:82
  430.8 1.3 reduce_sum.42
  (169 shorter events, 17.6 us)
Async XLA Ops:
  6.5 338.2 %copy-start = (bf16[2,256,256]{2,1,0:T(8,128)(2,1)S(1)}, bf16[2,256,256]{2,1,0:T(8,128)(2,1)}, u32[]{:S(2)}) copy-start(bf16[2,256,256]{2,1,0:T(8,128)(2,1)} %param.29) | copy-start | bytes 786436
  16.5 8.9 %copy-start.19 = (bf16[4096]{0:T(1024)(128)(2,1)S(1)}, bf16[4096]{0:T(1024)(128)(2,1)}, u32[]{:S(2)}) copy-start(bf16[4096]{0:T(1024)(128)(2,1)} %param.19) | copy-start | bytes 24580
  16.5 8.9 %copy-start.4 = (bf16[48,4096]{1,0:T(8,128)(2,1)S(1)}, bf16[48,4096]{1,0:T(8,128)(2,1)}, u32[]{:S(2)}) copy-start(bf16[48,4096]{1,0:T(8,128)(2,1)} %param.18) | copy-start | bytes 1179652
  16.5 9.3 %copy-start.7 = (bf16[4096,16]{0,1:T(8,128)(2,1)S(1)}, bf16[4096,16]{0,1:T(8,128)(2,1)}, u32[]{:S(2)}) copy-start(bf16[4096,16]{0,1:T(8,128)(2,1)} %param.22) | copy-start | bytes 393220
  16.5 9.6 %copy-start.8 = (bf16[4096,16]{0,1:T(8,128)(2,1)S(1)}, bf16[4096,16]{0,1:T(8,128)(2,1)}, u32[]{:S(2)}) copy-start(bf16[4096,16]{0,1:T(8,128)(2,1)} %param.23) | copy-start | bytes 393220
  16.6 257.9 %all-to-all-start = ((bf16[16,256,2048]{2,1,0:T(8,128)(2,1)}), bf16[16,256,2048]{2,1,0:T(8,128)(2,1)}, u32[]{:S(2)}, u32[]{:S(2)}) async-start(bf16[16,256,2048]{2,1,0:T(8,128)(2,1)} %stack.2), calls=%async_computation | async-start | bytes 33554432 | tf_op jit(solution)/shard_map/all_to_all | solution.py:26
  25.3 50.8 %all-gather.9.cloned.1.call-start = ((), (), s32[]{:S(2)}) async-start(), calls=%async_computation.2 | async-start | bytes 3649536 | tf_op jit(solution)/shard_map/all_gather | solution.py:44
  27.3 311.2 %all-gather.13.cloned.1.call-start = ((), (), s32[]{:S(2)}) async-start(), calls=%async_computation.4 | async-start | bytes 2621440 | tf_op jit(solution)/shard_map/all_gather | solution.py:64
  53.1 17.3 %copy-start.34 = (f32[16]{0:T(128)S(1)}, f32[16]{0:T(128)}, u32[]{:S(2)}) copy-start(f32[16]{0:T(128)} %param.24) | copy-start | bytes 196
  53.2 17.4 %copy-start.35 = (u32[128]{0:T(128)S(1)}, u32[128]{0:T(128)}, u32[]{:S(2)}) copy-start(u32[128]{0:T(128)} %constant.147) | copy-start | bytes 1540
  53.2 24.1 %copy-start.30 = (f32[384,2]{0,1:T(2,128)S(1)}, f32[384,2]{0,1:T(2,128)}, u32[]{:S(2)}) copy-start(f32[384,2]{0,1:T(2,128)} %param.25) | copy-start | bytes 9220
  78.6 202.1 %copy-start.13 = (f32[3,2]{1,0:T(4,128)}, f32[3,2]{1,0:T(4,128)S(1)}, u32[]{:S(2)}) copy-start(f32[3,2]{1,0:T(4,128)S(1)} %copy.151) | copy-start | bytes 76
  78.7 202.0 %copy-start.10 = (f32[384,2]{0,1:T(2,128)}, f32[384,2]{0,1:T(2,128)S(1)}, u32[]{:S(2)}) copy-start(f32[384,2]{0,1:T(2,128)S(1)} %copy.178) | copy-start | bytes 9220
  78.9 201.9 %copy-start.12 = (f32[3,2]{1,0:T(4,128)}, f32[3,2]{1,0:T(4,128)S(1)}, u32[]{:S(2)}) copy-start(f32[3,2]{1,0:T(4,128)S(1)} %add_reduce_fusion) | copy-start | bytes 76
  279.4 2.2 collective-permute-start.1
  300.3 0.8 copy-start.1
  301.1 75.2 %all-gather.11.cloned.1.call-start = ((), (), s32[]{:S(2)}) async-start(), calls=%async_computation.3 | async-start | bytes 2621440 | tf_op jit(solution)/shard_map/all_gather | solution.py:64
  302.4 5.0 %copy-start.14 = (f32[2]{0:T(128)S(1)}, f32[2]{0:T(128)}, u32[]{:S(2)}) copy-start(f32[2]{0:T(128)} %get-tuple-element.63) | copy-start | bytes 28
  302.4 33.9 %copy-start.5 = (bf16[2,256,256]{2,1,0:T(8,128)(2,1)S(1)}, bf16[2,256,256]{2,1,0:T(8,128)(2,1)}, u32[]{:S(2)}) copy-start(bf16[2,256,256]{2,1,0:T(8,128)(2,1)} %convert_element_type.135) | copy-start | bytes 786436
  302.5 34.5 %copy-start.20 = (f32[3,2]{1,0:T(4,128)S(1)}, f32[3,2]{1,0:T(4,128)}, u32[]{:S(2)}) copy-start(f32[3,2]{1,0:T(4,128)} %get-tuple-element.65) | copy-start | bytes 76
  302.5 34.5 %copy-start.31 = (f32[3,2]{1,0:T(4,128)S(1)}, f32[3,2]{1,0:T(4,128)}, u32[]{:S(2)}) copy-start(f32[3,2]{1,0:T(4,128)} %get-tuple-element.62) | copy-start | bytes 76
  307.4 33.7 %copy-start.9 = (pred[128,128]{1,0:T(8,128)(4,1)S(1)}, pred[128,128]{1,0:T(8,128)(4,1)}, u32[]{:S(2)}) copy-start(pred[128,128]{1,0:T(8,128)(4,1)} %iota_compare_fusion) | copy-start | bytes 49156
  307.4 33.7 %copy-start.11 = (f32[384,2]{0,1:T(2,128)S(1)}, f32[384,2]{0,1:T(2,128)}, u32[]{:S(2)}) copy-start(f32[384,2]{0,1:T(2,128)} %copy-done.10) | copy-start | bytes 9220
  307.9 35.1 %collective-permute-start = (bf16[16,512]{1,0:T(8,128)(2,1)S(1)}, bf16[16,512]{1,0:T(8,128)(2,1)S(1)}, u32[]{:S(2)}, u32[]{:S(2)}) collective-permute-start(bf16[16,512]{1,0:T(8,128)(2,1)S(1)} %slice.225), channel_id=1, source_target_pairs={{0,8},{8,16},{16,24},{24,32},{32,40},{40,48},{48,56},{56,64},{64,7... | collective-permute-start | bytes 49160 | tf_op jit(solution)/shard_map/ppermute | solution.py:50
  338.3 4.9 %copy-start.21 = (f32[2]{0:T(128)}, f32[2]{0:T(128)S(1)}, u32[]{:S(2)}) copy-start(f32[2]{0:T(128)S(1)} %get-tuple-element.215) | copy-start | bytes 28
  338.3 4.9 %copy-start.23 = (f32[2]{0:T(128)}, f32[2]{0:T(128)S(1)}, u32[]{:S(2)}) copy-start(f32[2]{0:T(128)S(1)} %get-tuple-element.216) | copy-start | bytes 28
  338.3 4.9 %copy-start.24 = (f32[2]{0:T(128)}, f32[2]{0:T(128)S(1)}, u32[]{:S(2)}) copy-start(f32[2]{0:T(128)S(1)} %get-tuple-element.217) | copy-start | bytes 28
  338.3 4.9 %copy-start.25 = (f32[2]{0:T(128)}, f32[2]{0:T(128)S(1)}, u32[]{:S(2)}) copy-start(f32[2]{0:T(128)S(1)} %get-tuple-element.218) | copy-start | bytes 28
  338.3 4.9 %copy-start.26 = (f32[2]{0:T(128)}, f32[2]{0:T(128)S(1)}, u32[]{:S(2)}) copy-start(f32[2]{0:T(128)S(1)} %get-tuple-element.219) | copy-start | bytes 28
  338.3 4.9 %copy-start.27 = (f32[2]{0:T(128)}, f32[2]{0:T(128)S(1)}, u32[]{:S(2)}) copy-start(f32[2]{0:T(128)S(1)} %get-tuple-element.220) | copy-start | bytes 28
  338.3 4.9 %copy-start.28 = (f32[2]{0:T(128)}, f32[2]{0:T(128)S(1)}, u32[]{:S(2)}) copy-start(f32[2]{0:T(128)S(1)} %get-tuple-element.221) | copy-start | bytes 28
  338.3 4.9 %copy-start.29 = (f32[2]{0:T(128)}, f32[2]{0:T(128)S(1)}, u32[]{:S(2)}) copy-start(f32[2]{0:T(128)S(1)} %get-tuple-element.222) | copy-start | bytes 28
  343.5 0.7 copy-start.15
  343.5 0.7 copy-start.16
  343.5 0.7 copy-start.32
  343.5 0.7 copy-start.33
  343.8 1.2 copy-start.18
  345.2 31.1 %copy-start.2 = (f32[8,256,256]{2,1,0:T(8,128)S(1)}, f32[8,256,256]{2,1,0:T(8,128)}, u32[]{:S(2)}) copy-start(f32[8,256,256]{2,1,0:T(8,128)} %all-gather.13.cloned.1.call-done) | copy-start | bytes 6291460
  345.2 31.1 %copy-start.22 = (f32[2]{0:T(128)S(1)}, f32[2]{0:T(128)}, u32[]{:S(2)}) copy-start(f32[2]{0:T(128)} %copy-done.21) | copy-start | bytes 28
  352.1 26.6 %copy-start.6 = (f32[3,128,2,256]{1,3,2,0:T(8,128)S(1)}, f32[3,128,2,256]{1,3,2,0:T(8,128)}, u32[]{:S(2)}) copy-start(f32[3,128,2,256]{1,3,2,0:T(8,128)} %convolution_bitcast_fusion) | copy-start | bytes 2359300
  376.3 2.4 copy-start.3
  381.8 0.8 copy-start.17
Sparse Core Ops, SparseCore 0:
  27.8 30.2 all-gather.8
  301.2 34.6 all-gather.12
  341.2 35.0 all-gather.10
